TPU v7x, 512 devices: a whole 4x8x8 slice. The times are simulated.
512 devices in a mesh: sp: 64 (over z, y), tp: 8 (over x, core).
Axes of the slice: x: 4, y: 8, z: 8, core: 2. Of those that a mesh axis runs over, the one named last changes fastest.
Arguments:
- queries: bfloat16 [16384, 1024], P('sp', 'tp'), may hold values from -6 to 6
- keys: bfloat16 [16384, 256], P('sp'), may hold values from -6 to 6
- values: bfloat16 [16384, 256], P('sp'), may hold values from -6 to 6
- query_gain: float32 [128], replicated, may hold values from 1.4 to 5.5
- key_gain: float32 [128], replicated, may hold values from 1.4 to 5.5
- residual_in: bfloat16 [16384, 2048], P(('sp', 'tp')), may hold values from -6 to 6
- out_weight: bfloat16 [1024, 2048], P('tp'), may hold values from -0.1875 to 0.1875
- norm_gain: float32 [2048], replicated, may hold values from 0.1 to 1.9
- gate_weight: bfloat16 [2048, 3072], P('sp', 'tp'), may hold values from -0.125 to 0.125
- up_weight: bfloat16 [2048, 3072], P('sp', 'tp'), may hold values from -0.125 to 0.125
- down_weight: bfloat16 [3072, 2048], P('tp', 'sp'), may hold values from -0.109375 to 0.109375
Outputs:
- result: bfloat16 [16384, 2048], P(('sp', 'tp'))
All inputs are finite; a program needn't handle non-finite values.
Results may differ from a plain program's by a relative error of at most 0.017.
Values may be sent and summed in bfloat16 or wider, within the bound.
A program may use at most 64 MiB of HBM per device.

v0:
```python
import math
import jax
import jax.numpy as jnp
from jax import lax
from jax.sharding import Mesh
from jax.sharding import PartitionSpec as P

Q_HEADS = 8
KV_HEADS = 2
GRID_WIDTH = 64
SP = ("sp_0", "sp_1")
SP_TP = ("sp_0", "sp_1", "tp")
EPS = 1e-06
ROPE_BASE = 10000.0


def side_by_side(arrays, axis, dim, along):
    widths = [a.shape[along] for a in arrays]
    both = jnp.concatenate(arrays, axis=along)
    result = lax.all_gather(both, axis, axis=dim, tiled=True)
    return tuple(jnp.split(result, [sum(widths[:k]) for k in range(1, len(widths))], axis=along))


def in_order(parts, dim):
    parts = jnp.moveaxis(parts, 0, dim)
    dims = parts.shape
    return parts.reshape(*dims[:dim], dims[dim] * dims[dim + 1], *dims[dim + 2 :])


def stacked_from(value, axes, turns):
    parts = value[None]
    for k in turns:
        parts = lax.all_gather(parts, axes[k], axis=0, tiled=True)
    block = [lax.axis_size(axes[k]) for k in reversed(turns)]
    parts = parts.reshape(*block, *value.shape)
    turned = sorted(range(len(turns)), key=lambda place: turns[len(turns) - 1 - place])
    return parts.transpose(*turned, *range(len(turns), parts.ndim)).reshape(-1, *value.shape)


def whole_of(value, axes, turns, dim):
    return in_order(stacked_from(value, axes, turns), dim)


def split_up(value, dim, size):
    before, after = (value.shape[:dim], value.shape[dim + 1 :])
    return jnp.moveaxis(value.reshape(*before, size, -1, *after), dim, 0)


def sent_and_summed(value, axis, dim):
    parts = split_up(value, dim, lax.axis_size(axis))
    arrived = lax.all_to_all(parts, axis, split_axis=0, concat_axis=0, tiled=True)
    return arrived.astype(jnp.float32).sum(axis=0)


def sent_to_all(value, axis):
    size = lax.axis_size(axis)
    return lax.all_to_all(
        jnp.broadcast_to(value[None], (size, *value.shape)), axis, 0, 0, tiled=True
    )


def gather_directly(value, axis, dim):
    return in_order(sent_to_all(value, axis), dim)


def normalize(wide_values, gain):
    wide = wide_values.astype(jnp.float32)
    return wide * lax.rsqrt(jnp.mean(wide * wide, axis=-1, keepdims=True) + EPS) * gain


def rotate_pair(segment, angles):
    half_size = segment.shape[-1] // 2
    first = segment[..., :half_size]
    second = segment[..., half_size:]
    cosine = jnp.cos(angles)[:, None, :]
    sine_part = jnp.sin(angles)[:, None, :]
    return jnp.concatenate(
        [first * cosine - second * sine_part, second * cosine + first * sine_part], axis=-1
    )


def grid_rotary(head_rows, positions):
    head_size = head_rows.shape[-1]
    half_size = head_size // 2
    quarter = head_size // 4
    inverse = ROPE_BASE ** (-jnp.arange(quarter, dtype=jnp.float32) * 2.0 / half_size)
    row_angles = (positions // GRID_WIDTH).astype(jnp.float32)[:, None] * inverse
    col_angles = (positions % GRID_WIDTH).astype(jnp.float32)[:, None] * inverse
    return jnp.concatenate(
        [
            rotate_pair(head_rows[..., :half_size], row_angles),
            rotate_pair(head_rows[..., half_size:], col_angles),
        ],
        axis=-1,
    )


def gated(gate_part, lifted):
    return (jax.nn.silu(gate_part) * lifted).astype(jnp.bfloat16)


def local(
    queries,
    keys,
    values,
    query_gain,
    key_gain,
    residual_in,
    out_weight,
    norm_gain,
    gate_weight,
    up_weight,
    down_weight,
):
    tok_rows = queries.shape[0]
    head_size = query_gain.shape[0]
    local_heads = queries.shape[1] // head_size
    tp_index = lax.axis_index("tp")
    gate_full, up_full = side_by_side((gate_weight, up_weight), SP, 0, 1)
    down_full = whole_of(down_weight, SP, (0, 1), 1)
    positions = lax.axis_index(SP) * tok_rows + jnp.arange(tok_rows, dtype=jnp.int32)
    key_head = tp_index * local_heads // (Q_HEADS // KV_HEADS)
    own_keys = lax.dynamic_slice_in_dim(keys, key_head * head_size, head_size, 1)
    own_values = lax.dynamic_slice_in_dim(values, key_head * head_size, head_size, 1)
    turned_keys = grid_rotary(
        normalize(own_keys.reshape(tok_rows, 1, head_size), key_gain), positions
    )
    turned_keys = turned_keys.reshape(tok_rows, head_size).astype(jnp.bfloat16)
    turned_queries = grid_rotary(
        normalize(queries.reshape(tok_rows, local_heads, head_size), query_gain), positions
    )
    turned_queries = turned_queries.reshape(tok_rows * local_heads, head_size).astype(jnp.bfloat16)
    score_scale = head_size ** (-0.5)

    def attend_block(running, block_pair):
        peak_score, weight_total, weighted = running
        block_keys, block_values = block_pair
        scores = (
            lax.dot_general(
                turned_queries,
                block_keys,
                (((1,), (1,)), ((), ())),
                preferred_element_type=jnp.float32,
            )
            * score_scale
        )
        new_peak = jnp.maximum(peak_score, jnp.max(scores, axis=1))
        factor = jnp.exp(peak_score - new_peak)
        raw = jnp.exp(scores - new_peak[:, None])
        weight_total = weight_total * factor + jnp.sum(raw, axis=1)
        weighted = weighted * factor[:, None] + jnp.dot(
            raw.astype(jnp.bfloat16), block_values, preferred_element_type=jnp.float32
        )
        return ((new_peak, weight_total, weighted), None)

    row_count = tok_rows * local_heads
    start_carry = (
        jnp.full((row_count,), -1e30, jnp.float32),
        jnp.zeros((row_count,), jnp.float32),
        jnp.zeros((row_count, head_size), jnp.float32),
    )
    piece_keys, piece_values = side_by_side((turned_keys, own_values), SP, 0, 1)
    span = math.gcd(piece_keys.shape[0], 512)
    blocks = piece_keys.shape[0] // span
    stacked = (
        piece_keys.reshape(blocks, span, head_size),
        piece_values.reshape(blocks, span, head_size),
    )
    updated, unused = lax.scan(attend_block, start_carry, stacked)
    peak_score, weight_total, weighted = updated
    attended = (weighted / weight_total[:, None]).astype(jnp.bfloat16)
    attention_out = sent_and_summed(
        jnp.dot(attended, out_weight, preferred_element_type=jnp.float32).astype(jnp.bfloat16),
        "tp",
        0,
    )
    middle = (residual_in.astype(jnp.float32) + attention_out).astype(jnp.bfloat16)
    normed = gather_directly(normalize(middle, norm_gain).astype(jnp.bfloat16), "tp", 0)
    hidden = gated(
        jnp.dot(normed, gate_full, preferred_element_type=jnp.float32),
        jnp.dot(normed, up_full, preferred_element_type=jnp.float32),
    )
    partials = jnp.dot(hidden, down_full, preferred_element_type=jnp.float32)
    mixer_out = sent_and_summed(partials.astype(jnp.bfloat16), "tp", 0)
    return (middle.astype(jnp.float32) + mixer_out).astype(jnp.bfloat16)


def solution(mesh):
    finer = Mesh(mesh.devices.reshape(8, 8, mesh.shape["tp"]), ("sp_0", "sp_1", "tp"))
    in_specs = (
        P(SP, "tp"),
        P(SP, None),
        P(SP, None),
        P(),
        P(),
        P(SP_TP, None),
        P("tp", None),
        P(),
        P(SP, "tp"),
        P(SP, "tp"),
        P("tp", SP),
    )
    out_specs = P(SP_TP, None)
    return jax.shard_map(local, mesh=finer, in_specs=in_specs, out_specs=out_specs, check_vma=False)
```

profile of v0, /device:TPU:1, one launch (start us, length us, event | category | flops | bytes accessed | tf_op | source)
XLA Modules:
  0.0 299.4 jit_solution(13438292741110055341)
XLA Ops:
  11.4 26.1 %all-gather = bf16[3072,32]{0,1:T(8,128)(2,1)S(1)} all-gather(bf16[384,32]{0,1:T(8,128)(2,1)} %param.23), channel_id=2, replica_groups=mesh['sp_0'=8,'sp_1'=8,'tp'=8] {'sp_0'}, dimensions={0}, use_global_device_ids=true | all-gather | bytes 221184 | tf_op jit(solution)/shard_map/all_gather | solution.py:33
  38.2 1.4 pad_maximum_fusion.1
  39.8 80.1 %all-gather.5.cloned.1.call-done = bf16[16384,256]{0,1:T(8,128)(2,1)} async-done(((bf16[256,256]{0,1:T(8,128)(2,1)}), bf16[16384,256]{0,1:T(8,128)(2,1)}) %all-gather.5.cloned.1.call-update) | async-done | bytes 8388624 | tf_op jit(solution)/shard_map/all_gather | solution.py:20
  119.9 5.8 %fusion.78 = (bf16[16384,128]{0,1:T(8,128)(2,1)}, bf16[16384,128]{0,1:T(8,128)(2,1)}) fusion(bf16[16384,256]{0,1:T(8,128)(2,1)} %all-gather.5.cloned.1.call-done), kind=kLoop, calls=%fused_computation.112 | loop fusion | bytes 16777216 | tf_op jit(solution)/shard_map/split | solution.py:21
  125.7 6.4 %copy.23 = bf16[16384,128]{1,0:T(8,128)(2,1)} copy(bf16[16384,128]{0,1:T(8,128)(2,1)} %get-tuple-element.97) | data formatting | bytes 8388608
  132.0 6.4 %copy.24 = bf16[16384,128]{1,0:T(8,128)(2,1)} copy(bf16[16384,128]{0,1:T(8,128)(2,1)} %get-tuple-element.96) | data formatting | bytes 8388608
  138.4 81.8 %while.15 = (s32[]{:T(128)}, f32[256]{0:T(256)S(1)}, f32[256]{0:T(256)S(1)}, f32[256,128]{1,0:T(8,128)S(1)}, bf16[32,512,128]{2,1,0:T(8,128)(2,1)}, /*index=5*/b...) while((s32[]{:T(128)}, f32[256]{0:T(256)S(1)}, ...), condition=%wide.region_5.6_spmd.clone, body=%wide.region_2.5_spmd.clone.sunk | while | flops 67994880 | bytes 2180201 | solution.py:169
  139.8 1.2 convolution_add_fusion.2
  142.3 1.2 convolution_add_fusion.2
  144.9 1.2 convolution_add_fusion.2
  147.4 1.2 convolution_add_fusion.2
  150.0 1.2 convolution_add_fusion.2
  151.2 1.2 fusion.94
  152.5 1.2 convolution_add_fusion.2
  155.1 1.2 convolution_add_fusion.2
  157.7 1.2 convolution_add_fusion.2
  160.2 1.2 convolution_add_fusion.2
  162.8 1.2 convolution_add_fusion.2
  165.3 1.2 convolution_add_fusion.2
  167.9 1.2 convolution_add_fusion.2
  170.4 1.2 convolution_add_fusion.2
  173.0 1.2 convolution_add_fusion.2
  175.6 1.2 convolution_add_fusion.2
  178.1 1.2 convolution_add_fusion.2
  180.7 1.2 convolution_add_fusion.2
  183.2 1.2 convolution_add_fusion.2
  185.8 1.2 convolution_add_fusion.2
  188.3 1.2 convolution_add_fusion.2
  190.9 1.2 convolution_add_fusion.2
  193.4 1.2 convolution_add_fusion.2
  194.7 1.2 fusion.94
  196.0 1.2 convolution_add_fusion.2
  198.6 1.2 convolution_add_fusion.2
  201.1 1.2 convolution_add_fusion.2
  203.7 1.2 convolution_add_fusion.2
  206.2 1.2 convolution_add_fusion.2
  208.8 1.2 convolution_add_fusion.2
  211.3 1.2 convolution_add_fusion.2
  213.9 1.2 convolution_add_fusion.2
  216.4 1.2 convolution_add_fusion.2
  219.0 1.2 convolution_add_fusion.2
  220.7 24.3 %all_to_all.15 = bf16[8,32,2048]{2,1,0:T(8,128)(2,1)S(1)} all-to-all(bf16[8,32,2048]{2,1,0:T(8,128)(2,1)S(1)} %bitcast.46), channel_id=1, replica_groups=mesh['sp_0'=8,'sp_1'=8,'tp'=8] {'tp'}, dimensions={0} | all-to-all | bytes 2097152 | tf_op jit(solution)/shard_map/all_to_all | solution.py:51
  246.6 4.5 %all-to-all-start.1 = ((bf16[8,32,2048]{2,1,0:T(8,128)(2,1)}), bf16[8,32,2048]{2,1,0:T(8,128)(2,1)S(1)}, u32[]{:S(2)}, u32[]{:S(2)}) async-start(bf16[8,32,2048]{2,1,0:T(8,128)(2,1)} %broadcast_in_dim.13), calls=%async_computation.1 | async-start | bytes 2097152 | tf_op jit(solution)/shard_map/all_to_all | solution.py:57
  251.1 2.3 copy.22
  253.4 12.6 %all-to-all-done.1 = bf16[8,32,2048]{2,1,0:T(8,128)(2,1)S(1)} async-done(((bf16[8,32,2048]{2,1,0:T(8,128)(2,1)}), bf16[8,32,2048]{2,1,0:T(8,128)(2,1)S(1)}, u32[]{:S(2)}, u32[]{:S(2)}) %all-to-all-start.1) | async-done | bytes 1048608 | tf_op jit(solution)/shard_map/all_to_all | solution.py:57
  266.1 2.9 fusion.14
  268.9 3.8 %convolution_convert_fusion = bf16[256,2048]{1,0:T(8,128)(2,1)} fusion(bf16[384,2048]{0,1:T(8,128)(2,1)S(1)} %bitcast.48, bf16[256,2048]{1,0:T(8,128)(2,1)S(1)} %bitcast.50, bf16[2048,768]{1,0:T(8,128)(2,1)} %all-gather.7.cloned.1.call-done, f32[256,384]{1,0:T(8,128)} %fusion.14), kind=kOutput, calls=%fused_computation.18 | convolution fusion | flops 806420480 | bytes 5636096 | tf_op jit(solution)/shard_map/dot_general | solution.py:183
  272.7 19.4 %all_to_all.16 = bf16[8,32,2048]{2,1,0:T(8,128)(2,1)S(1)} all-to-all(bf16[8,32,2048]{2,1,0:T(8,128)(2,1)} %bitcast.51), channel_id=1, replica_groups=mesh['sp_0'=8,'sp_1'=8,'tp'=8] {'tp'}, dimensions={0} | all-to-all | bytes 2097152 | tf_op jit(solution)/shard_map/all_to_all | solution.py:51
  (201 shorter events, 48.3 us)
Async XLA Ops:
  6.5 213.7 %copy-start = (bf16[128,2048]{1,0:T(8,128)(2,1)S(1)}, bf16[128,2048]{1,0:T(8,128)(2,1)}, u32[]{:S(2)}) copy-start(bf16[128,2048]{1,0:T(8,128)(2,1)} %param.19) | copy-start | bytes 1572868
  6.5 113.3 %all-gather.5.cloned.1.call-start = ((), (), s32[]{:S(2)}) async-start(), calls=%async_computation.3 | async-start | bytes 8519680 | tf_op jit(solution)/shard_map/all_gather | solution.py:20
  11.3 239.7 %all-gather.9.cloned.1.call-start = ((), (), s32[]{:S(2)}) async-start(), calls=%async_computation.5 | async-start | bytes 1769472 | tf_op jit(solution)/shard_map/all_gather | solution.py:33
  38.2 215.2 %all-gather.7.cloned.1.call-start = ((), (), s32[]{:S(2)}) async-start(), calls=%async_computation.4 | async-start | bytes 3194880 | tf_op jit(solution)/shard_map/all_gather | solution.py:20
  220.2 25.0 %copy-start.1 = (bf16[32,2048]{1,0:T(8,128)(2,1)S(1)}, bf16[32,2048]{1,0:T(8,128)(2,1)}, u32[]{:S(2)}) copy-start(bf16[32,2048]{1,0:T(8,128)(2,1)} %param.18) | copy-start | bytes 393220
  220.2 25.1 %copy-start.2 = (f32[2048]{0:T(1024)S(1)}, f32[2048]{0:T(1024)}, u32[]{:S(2)}) copy-start(f32[2048]{0:T(1024)} %param.20) | copy-start | bytes 24580
  246.6 19.5 %all-to-all-start.1 = ((bf16[8,32,2048]{2,1,0:T(8,128)(2,1)}), bf16[8,32,2048]{2,1,0:T(8,128)(2,1)S(1)}, u32[]{:S(2)}, u32[]{:S(2)}) async-start(bf16[8,32,2048]{2,1,0:T(8,128)(2,1)} %broadcast_in_dim.13), calls=%async_computation.1 | async-start | bytes 2097152 | tf_op jit(solution)/shard_map/all_to_all | solution.py:57
Sparse Core Ops, SparseCore 0:
  11.5 108.3 all-gather.4
  122.0 38.1 all-gather.8
  163.1 85.2 all-gather.6
where the time goes:
time: 301 us; the launch traced here: 299 us
  waiting for transfers between devices  92.8 us (31%)
  matrix products  82.6 us (27%)
  blocking collectives  69.7 us (23%)
  local copies, waits for them, and re-layouts  25 us (8%)
  between operations  13.3 us (4%)
  other arithmetic  9.95 us (3%)
  starting transfers between devices  4.58 us (2%)
    all_gather x2, waiting for transfers between devices, side_by_side(): result = lax.all_gather(both, axis, axis=dim, tiled=True)  80.1 us
    all_to_all x2, blocking collectives, sent_and_summed(): lax.all_to_all(parts, axis, split_axis=0, concat_axis=0, tiled=True)  43.7 us
    dot_general x32, matrix products, attend_block(): jnp.dot(raw.astype(jnp.bfloat16), block_values, preferred_element_type=jn...  38.1 us
    dot_general x32, matrix products, attend_block(): lax.dot_general(turned_queries, block_keys, (((1,), (1,)), ((), ())), pre...  37.4 us
    all_gather x1, blocking collectives, stacked_from(): parts = lax.all_gather(parts, axes[k], axis=0, tiled=True)  26.1 us
    unnamed x13, local copies, waits for them, and re-layouts  14.7 us
    all_to_all x1, waiting for transfers between devices, sent_to_all(): lax.all_to_all(jnp.broadcast_to(value[None], (size, *value.shape)), axis,...  12.6 us
  transfers between devices with their start and end apart: 4, of which 2 were waited for; matrix products, arithmetic and copies ran while one was open for 35% of the time, Pallas kernels for 0%

commit v1 on v0

--- a/solution.py
+++ b/solution.py
@@ -30,7 +30,9 @@
 def stacked_from(value, axes, turns):
     parts = value[None]
     for k in turns:
-        parts = lax.all_gather(parts, axes[k], axis=0, tiled=True)
+        parts = jnp.concatenate(
+            lax.all_to_all(jnp.stack([parts] * lax.axis_size(axes[k])), axes[k], 0, 0), axis=0
+        )
     block = [lax.axis_size(axes[k]) for k in reversed(turns)]
     parts = parts.reshape(*block, *value.shape)
     turned = sorted(range(len(turns)), key=lambda place: turns[len(turns) - 1 - place])

time: 301 us -> 348 us (1.16)
  waiting for transfers between devices: 92.8 us -> 148 us
  blocking collectives: 69.7 us -> 43.9 us
  starting transfers between devices: 4.58 us -> 19.3 us
    all_to_all x0 -> x2, waiting for transfers between devices: none -> 40 us  [stacked_from(): lax.all_to_all(jnp.stack([parts] * lax.axis_size(axes[k])), axes[k], 0, 0)]
    all_gather x1 -> x0, blocking collectives: 26.1 us -> none  [stacked_from(): parts = lax.all_gather(parts, axes[k], axis=0, tiled=True)]
    all_to_all x0 -> x2, starting transfers between devices: none -> 15.2 us  [stacked_from(): lax.all_to_all(jnp.stack([parts] * lax.axis_size(axes[k])), axes[k], 0, 0)]
    all_gather x2, waiting for transfers between devices: 80.1 us -> 94.6 us  [side_by_side(): result = lax.all_gather(both, axis, axis=dim, tiled=True)]
    unnamed x13 -> x14, local copies, waits for them, and re-layouts: 14.7 us -> 14.1 us
  transfers between devices with their start and end apart: 4 -> 5, of which waited for: 2 -> 3; matrix products, arithmetic and copies ran while one was open for 35% -> 31% of each run, Pallas kernels for 0% -> 0%
where the time goes in v1:
time: 348 us; the launch traced here: 346 us
  waiting for transfers between devices  148 us (43%)
  matrix products  83.6 us (24%)
  blocking collectives  43.9 us (13%)
  local copies, waits for them, and re-layouts  26.1 us (8%)
  starting transfers between devices  19.3 us (6%)
  between operations  13.6 us (4%)
  other arithmetic  9.94 us (3%)
    all_gather x2, waiting for transfers between devices, side_by_side(): result = lax.all_gather(both, axis, axis=dim, tiled=True)  94.6 us
    all_to_all x2, blocking collectives, sent_and_summed(): lax.all_to_all(parts, axis, split_axis=0, concat_axis=0, tiled=True)  43.9 us
    all_to_all x2, waiting for transfers between devices, stacked_from(): lax.all_to_all(jnp.stack([parts] * lax.axis_size(axes[k])), axes[k], 0, 0)  40 us
    dot_general x32, matrix products, attend_block(): jnp.dot(raw.astype(jnp.bfloat16), block_values, preferred_element_type=jn...  38.1 us
    dot_general x32, matrix products, attend_block(): lax.dot_general(turned_queries, block_keys, (((1,), (1,)), ((), ())), pre...  37.4 us
    all_to_all x2, starting transfers between devices, stacked_from(): lax.all_to_all(jnp.stack([parts] * lax.axis_size(axes[k])), axes[k], 0, 0)  15.2 us
    unnamed x14, local copies, waits for them, and re-layouts  14.1 us
    all_to_all x1, waiting for transfers between devices, sent_to_all(): lax.all_to_all(jnp.broadcast_to(value[None], (size, *value.shape)), axis,...  13.6 us
  transfers between devices with their start and end apart: 5, of which 3 were waited for; matrix products, arithmetic and copies ran while one was open for 31% of the time, Pallas kernels for 0%

profile of v1, /device:TPU:1, one launch (start us, length us, event | category | flops | bytes accessed | tf_op | source)
XLA Modules:
  0.0 346.0 jit_solution(15936420567894466784)
XLA Ops:
  11.3 1.4 stack.6
  12.8 10.9 %all-to-all-start.2 = ((bf16[8,1,384,32]{2,3,1,0:T(8,128)(2,1)}), bf16[8,1,384,32]{2,3,1,0:T(8,128)(2,1)S(1)}, u32[]{:S(2)}, u32[]{:S(2)}) async-start(bf16[8,1,384,32]{2,3,1,0:T(8,128)(2,1)} %stack.6), calls=%async_computation.2 | async-start | bytes 393216 | tf_op jit(solution)/shard_map/all_to_all | solution.py:34
  23.7 1.4 pad_maximum_fusion.1
  25.2 94.6 %all-gather.3.cloned.1.call-done = bf16[16384,256]{0,1:T(8,128)(2,1)} async-done(((bf16[256,256]{0,1:T(8,128)(2,1)}), bf16[16384,256]{0,1:T(8,128)(2,1)}) %all-gather.3.cloned.1.call-update) | async-done | bytes 8388624 | tf_op jit(solution)/shard_map/all_gather | solution.py:20
  119.9 5.8 %fusion.78 = (bf16[16384,128]{0,1:T(8,128)(2,1)}, bf16[16384,128]{0,1:T(8,128)(2,1)}) fusion(bf16[16384,256]{0,1:T(8,128)(2,1)} %all-gather.3.cloned.1.call-done), kind=kLoop, calls=%fused_computation.112 | loop fusion | bytes 16777216 | tf_op jit(solution)/shard_map/split | solution.py:21
  125.7 6.4 %copy.21 = bf16[16384,128]{1,0:T(8,128)(2,1)} copy(bf16[16384,128]{0,1:T(8,128)(2,1)} %get-tuple-element.97) | data formatting | bytes 8388608
  132.0 6.4 %copy.22 = bf16[16384,128]{1,0:T(8,128)(2,1)} copy(bf16[16384,128]{0,1:T(8,128)(2,1)} %get-tuple-element.96) | data formatting | bytes 8388608
  138.4 81.7 %while.15 = (s32[]{:T(128)}, f32[256]{0:T(256)S(1)}, f32[256]{0:T(256)S(1)}, f32[256,128]{1,0:T(8,128)S(1)}, bf16[32,512,128]{2,1,0:T(8,128)(2,1)}, /*index=5*/b...) while((s32[]{:T(128)}, f32[256]{0:T(256)S(1)}, ...), condition=%wide.region_5.6_spmd.clone, body=%wide.region_2.5_spmd.clone.sunk | while | flops 67994880 | bytes 2180201 | solution.py:171
  139.8 1.2 convolution_add_fusion.2
  142.3 1.2 convolution_add_fusion.2
  144.9 1.2 convolution_add_fusion.2
  147.4 1.2 convolution_add_fusion.2
  150.0 1.2 convolution_add_fusion.2
  152.5 1.2 convolution_add_fusion.2
  155.1 1.2 convolution_add_fusion.2
  157.6 1.2 convolution_add_fusion.2
  160.2 1.2 convolution_add_fusion.2
  162.7 1.2 convolution_add_fusion.2
  165.3 1.2 convolution_add_fusion.2
  167.8 1.2 convolution_add_fusion.2
  170.4 1.2 convolution_add_fusion.2
  172.9 1.2 convolution_add_fusion.2
  175.5 1.2 convolution_add_fusion.2
  178.0 1.2 convolution_add_fusion.2
  180.6 1.2 convolution_add_fusion.2
  183.2 1.2 convolution_add_fusion.2
  185.7 1.2 convolution_add_fusion.2
  188.3 1.2 convolution_add_fusion.2
  190.8 1.2 convolution_add_fusion.2
  193.4 1.2 convolution_add_fusion.2
  195.9 1.2 convolution_add_fusion.2
  198.5 1.2 convolution_add_fusion.2
  201.1 1.2 convolution_add_fusion.2
  203.6 1.2 convolution_add_fusion.2
  206.2 1.2 convolution_add_fusion.2
  208.7 1.2 convolution_add_fusion.2
  211.3 1.2 convolution_add_fusion.2
  220.1 1.5 convolution_convert_fusion.1
  221.6 24.5 %all_to_all.25 = bf16[8,32,2048]{2,1,0:T(8,128)(2,1)S(1)} all-to-all(bf16[8,32,2048]{2,1,0:T(8,128)(2,1)} %bitcast.42), channel_id=1, replica_groups=mesh['sp_0'=8,'sp_1'=8,'tp'=8] {'tp'}, dimensions={0} | all-to-all | bytes 2097152 | tf_op jit(solution)/shard_map/all_to_all | solution.py:53
  246.1 1.3 stack.7
  247.5 4.4 %all-to-all-start.3 = ((bf16[8,8,384,32]{2,3,1,0:T(8,128)(2,1)}), bf16[8,8,384,32]{2,3,1,0:T(8,128)(2,1)S(1)}, u32[]{:S(2)}, u32[]{:S(2)}) async-start(bf16[8,8,384,32]{2,3,1,0:T(8,128)(2,1)} %stack.7), calls=%async_computation.3 | async-start | bytes 3145728 | tf_op jit(solution)/shard_map/all_to_all | solution.py:34
  252.3 40.0 %all-to-all-done.3 = bf16[8,8,384,32]{2,3,1,0:T(8,128)(2,1)S(1)} async-done(((bf16[8,8,384,32]{2,3,1,0:T(8,128)(2,1)}), bf16[8,8,384,32]{2,3,1,0:T(8,128)(2,1)S(1)}, u32[]{:S(2)}, u32[]{:S(2)}) %all-to-all-start.3) | async-done | bytes 1572896 | tf_op jit(solution)/shard_map/all_to_all | solution.py:34
  293.4 4.0 %all-to-all-start.1 = ((bf16[8,32,2048]{2,1,0:T(8,128)(2,1)}), bf16[8,32,2048]{2,1,0:T(8,128)(2,1)S(1)}, u32[]{:S(2)}, u32[]{:S(2)}) async-start(bf16[8,32,2048]{2,1,0:T(8,128)(2,1)} %broadcast_in_dim.11), calls=%async_computation.1 | async-start | bytes 2097152 | tf_op jit(solution)/shard_map/all_to_all | solution.py:59
  297.4 1.4 copy.20
  298.7 13.6 %all-to-all-done.1 = bf16[8,32,2048]{2,1,0:T(8,128)(2,1)S(1)} async-done(((bf16[8,32,2048]{2,1,0:T(8,128)(2,1)}), bf16[8,32,2048]{2,1,0:T(8,128)(2,1)S(1)}, u32[]{:S(2)}, u32[]{:S(2)}) %all-to-all-start.1) | async-done | bytes 1048608 | tf_op jit(solution)/shard_map/all_to_all | solution.py:59
  312.4 2.9 fusion.14
  315.2 3.8 %convolution_convert_fusion = bf16[256,2048]{1,0:T(8,128)(2,1)} fusion(bf16[384,2048]{0,1:T(8,128)(2,1)S(1)} %bitcast.43, bf16[256,2048]{1,0:T(8,128)(2,1)S(1)} %bitcast.45, bf16[2048,768]{1,0:T(8,128)(2,1)} %all-gather.5.cloned.1.call-done, f32[256,384]{1,0:T(8,128)} %fusion.14), kind=kOutput, calls=%fused_computation.18 | convolution fusion | flops 806420480 | bytes 5636096 | tf_op jit(solution)/shard_map/dot_general | solution.py:185
  319.0 19.4 %all_to_all.26 = bf16[8,32,2048]{2,1,0:T(8,128)(2,1)S(1)} all-to-all(bf16[8,32,2048]{2,1,0:T(8,128)(2,1)} %bitcast.46), channel_id=1, replica_groups=mesh['sp_0'=8,'sp_1'=8,'tp'=8] {'tp'}, dimensions={0} | all-to-all | bytes 2097152 | tf_op jit(solution)/shard_map/all_to_all | solution.py:53
  (204 shorter events, 53.0 us)
Async XLA Ops:
  6.5 213.6 %copy-start = (bf16[128,2048]{1,0:T(8,128)(2,1)S(1)}, bf16[128,2048]{1,0:T(8,128)(2,1)}, u32[]{:S(2)}) copy-start(bf16[128,2048]{1,0:T(8,128)(2,1)} %param.19) | copy-start | bytes 1572868
  6.5 113.3 %all-gather.3.cloned.1.call-start = ((), (), s32[]{:S(2)}) async-start(), calls=%async_computation.5 | async-start | bytes 8519680 | tf_op jit(solution)/shard_map/all_gather | solution.py:20
  12.8 208.8 %all-to-all-start.2 = ((bf16[8,1,384,32]{2,3,1,0:T(8,128)(2,1)}), bf16[8,1,384,32]{2,3,1,0:T(8,128)(2,1)S(1)}, u32[]{:S(2)}, u32[]{:S(2)}) async-start(bf16[8,1,384,32]{2,3,1,0:T(8,128)(2,1)} %stack.6), calls=%async_computation.2 | async-start | bytes 393216 | tf_op jit(solution)/shard_map/all_to_all | solution.py:34
  23.6 275.1 %all-gather.5.cloned.1.call-start = ((), (), s32[]{:S(2)}) async-start(), calls=%async_computation.6 | async-start | bytes 3194880 | tf_op jit(solution)/shard_map/all_gather | solution.py:20
  246.1 5.9 %copy-start.2 = (bf16[32,2048]{1,0:T(8,128)(2,1)S(1)}, bf16[32,2048]{1,0:T(8,128)(2,1)}, u32[]{:S(2)}) copy-start(bf16[32,2048]{1,0:T(8,128)(2,1)} %param.18) | copy-start | bytes 393220
  246.1 6.1 %copy-start.3 = (f32[2048]{0:T(1024)S(1)}, f32[2048]{0:T(1024)}, u32[]{:S(2)}) copy-start(f32[2048]{0:T(1024)} %param.20) | copy-start | bytes 24580
  247.5 44.8 %all-to-all-start.3 = ((bf16[8,8,384,32]{2,3,1,0:T(8,128)(2,1)}), bf16[8,8,384,32]{2,3,1,0:T(8,128)(2,1)S(1)}, u32[]{:S(2)}, u32[]{:S(2)}) async-start(bf16[8,8,384,32]{2,3,1,0:T(8,128)(2,1)} %stack.7), calls=%async_computation.3 | async-start | bytes 3145728 | tf_op jit(solution)/shard_map/all_to_all | solution.py:34
  293.4 19.0 %all-to-all-start.1 = ((bf16[8,32,2048]{2,1,0:T(8,128)(2,1)}), bf16[8,32,2048]{2,1,0:T(8,128)(2,1)S(1)}, u32[]{:S(2)}, u32[]{:S(2)}) async-start(bf16[8,32,2048]{2,1,0:T(8,128)(2,1)} %broadcast_in_dim.11), calls=%async_computation.1 | async-start | bytes 2097152 | tf_op jit(solution)/shard_map/all_to_all | solution.py:59
  298.7 16.5 %copy-start.1 = (bf16[8,8,384,32]{2,3,0,1:T(8,128)(2,1)S(1)}, bf16[8,8,384,32]{2,3,0,1:T(8,128)(2,1)}, u32[]{:S(2)}) copy-start(bf16[8,8,384,32]{2,3,0,1:T(8,128)(2,1)} %copy.20) | copy-start | bytes 4718596
Sparse Core Ops, SparseCore 0:
  11.5 108.3 all-gather.2
  122.9 82.2 all-gather.4
